TPU v7x, 32 devices: a whole 2x2x4 slice. The times are simulated.
32 devices in a mesh: dp: 4 (over y, x), kv: 4 (over z), tp: 2 (over core).
Axes of the slice: x: 2, y: 2, z: 4, core: 2. Of those that a mesh axis runs over, the one named last changes fastest.
Arguments:
- tokens: bfloat16 [256, 2048], P('dp', ('kv', 'tp')), parts along dimension 0, may hold values from -64 to 64, as said below
- lengths: int32 [32], P(('dp', 'kv', 'tp')), parts along dimension 0, may hold values from 1 to 8, 28 in all
- state: float32 [32, 16, 128, 128], P(('dp', 'kv', 'tp')), parts along dimension 0, may hold values from -1.8 to 1.8
- gain_first: float32 [2048], replicated, may hold values from 0.1 to 1.9
- first_gate: bfloat16 [2048, 5632], P(None, 'kv'), may hold values from -0.125 to 0.125
- first_up: bfloat16 [2048, 5632], P(None, 'kv'), may hold values from -0.125 to 0.125
- first_down: bfloat16 [5632, 2048], P('kv'), may hold values from -0.109375 to 0.109375
- gain_mix: float32 [2048], replicated, may hold values from 0.1 to 1.9
- query_weight: bfloat16 [2048, 2048], P(None, ('kv', 'tp')), may hold values from -0.125 to 0.125
- key_weight: bfloat16 [2048, 2048], P(None, ('kv', 'tp')), may hold values from -0.125 to 0.125
- value_weight: bfloat16 [2048, 2048], P(None, ('kv', 'tp')), may hold values from -0.125 to 0.125
- gating_weight: bfloat16 [2048, 2048], P(None, ('kv', 'tp')), may hold values from -0.125 to 0.125
- write_weight: bfloat16 [2048, 16], replicated, may hold values from -0.125 to 0.125
- forget_weight: bfloat16 [2048, 16], replicated, may hold values from -0.125 to 0.125
- forget_rate: float32 [16], replicated, may hold values from -4 to 1.5
- out_weight: bfloat16 [2048, 2048], P(None, ('kv', 'tp')), may hold values from -0.125 to 0.125
- gain_second: float32 [2048], replicated, may hold values from 0.1 to 1.9
- second_gate: bfloat16 [2048, 5632], P(None, 'kv'), may hold values from -0.125 to 0.125
- second_up: bfloat16 [2048, 5632], P(None, 'kv'), may hold values from -0.125 to 0.125
- second_down: bfloat16 [5632, 2048], P('kv'), may hold values from -0.109375 to 0.109375
Outputs:
- mixed_out: bfloat16 [256, 2048], P('dp', ('kv', 'tp')), parts along dimension 0
- new_state: float32 [32, 16, 128, 128], P(('dp', 'kv', 'tp')), parts along dimension 0
There are 4 independent parts, one for each index of `dp`. A program takes and returns all parts, laid end to end along the dimension named above; an argument that names none is the same for every part. Nothing has to cross between parts.
Inputs may be any that keep to these rules, and one draw needn't show every extreme that they name: Activations of the new tokens. `lengths`: the live new tokens of each sequence; within each independent group of 8 sequences (one part along dp) they sum to seven halves of 8, rounded down, and some sequence of each group has all 8 live.
All inputs are finite; a program needn't handle non-finite values.
Results may differ from a plain program's by a relative error of at most 0.0058.
Values may be sent and summed in bfloat16 or wider, within the bound.
A program may use at most 128 MiB of HBM per device.

v0:
```python
import math
import jax
import jax.numpy as jnp
from jax import lax
from jax.sharding import PartitionSpec as P

HEADS = 16
HEAD = 128
BLK = 8
EPSILON = 1e-06


def fold_step(gain, gate_cols, up_cols, portion):
    values = portion.astype(jnp.float32)
    scaled = (values * gain).astype(jnp.bfloat16)
    gate_acc = jnp.dot(scaled, gate_cols, preferred_element_type=jnp.float32)
    up_acc = jnp.dot(scaled, up_cols, preferred_element_type=jnp.float32)
    squares = jnp.sum(values * values, axis=1)
    return (gate_acc, up_acc, squares)


def finish_units(gate_acc, up_acc, squares, channels, down_rows):
    row_scale = lax.rsqrt(squares / channels + EPSILON)[:, None]
    hidden = (jax.nn.silu(gate_acc * row_scale) * (up_acc * row_scale)).astype(jnp.bfloat16)
    return jnp.dot(hidden, down_rows, preferred_element_type=jnp.float32)


def feed_forward(hidden_in, gain, w_gate, w_up, w_down):
    channels = gain.shape[0]
    paired = lax.all_to_all(hidden_in, "tp", split_axis=0, concat_axis=1, tiled=True)
    gate_acc, up_acc, squares = fold_step(
        gain, w_gate, w_up, lax.all_gather(paired, "kv", axis=1, tiled=True)
    )
    ffn_term = finish_units(gate_acc, up_acc, squares, channels, w_down)
    partial_value = lax.psum_scatter(ffn_term, "kv", scatter_dimension=1, tiled=True)
    summed = lax.all_to_all(partial_value, "tp", split_axis=1, concat_axis=0, tiled=True)
    return (hidden_in.astype(jnp.float32) + 0.5 * summed).astype(jnp.bfloat16)


def delta_block(query, key_in, value, gating, write_pre, forget_pre, rates, live, state):
    seq_count, block_len, head_count, head_size = query.shape
    precise = lax.Precision.HIGHEST
    query_unit = (
        query
        * lax.rsqrt(jnp.sum(query * query, axis=-1, keepdims=True) + EPSILON)
        / math.sqrt(head_size)
    )
    key_unit = key_in * lax.rsqrt(jnp.sum(key_in * key_in, axis=-1, keepdims=True) + EPSILON)
    live_rows = live[:, :, None]
    write_gate = jax.nn.sigmoid(write_pre) * live_rows
    forget = -jnp.exp(rates)[None, None, :] * jax.nn.softplus(forget_pre) * live_rows
    cumulative = jnp.cumsum(forget, axis=1)
    cum_heads = jnp.transpose(cumulative, (0, 2, 1))
    positions = jnp.arange(block_len)
    causal = positions[:, None] >= positions[None, :]
    strict = positions[:, None] > positions[None, :]
    differ = jnp.minimum(cum_heads[:, :, :, None] - cum_heads[:, :, None, :], 0.0)
    decay_mat = jnp.where(causal, jnp.exp(differ), 0.0)
    key_dots = jnp.einsum("sthd,suhd->shtu", key_unit, key_unit, precision=precise)
    write_heads = jnp.transpose(write_gate, (0, 2, 1))
    strict_part = jnp.where(strict, write_heads[:, :, :, None] * decay_mat * key_dots, 0.0)
    identity = jnp.eye(block_len, dtype=jnp.float32)
    squared = jnp.einsum("shtu,shuv->shtv", strict_part, strict_part, precision=precise)
    fourth = jnp.einsum("shtu,shuv->shtv", squared, squared, precision=precise)
    inverse = jnp.einsum(
        "shtu,shuv->shtv", identity - strict_part, identity + squared, precision=precise
    )
    inverse = jnp.einsum("shtu,shuv->shtv", inverse, identity + fourth, precision=precise)
    growth = jnp.exp(cumulative)
    target = jnp.einsum(
        "shtu,suhv->sthv", inverse, write_gate[..., None] * value, precision=precise
    )
    key_mix = jnp.einsum(
        "shtu,suhk->sthk", inverse, (write_gate * growth)[..., None] * key_unit, precision=precise
    )
    update = target - jnp.einsum("sthk,shkv->sthv", key_mix, state, precision=precise)
    scores = jnp.einsum("sthd,suhd->shtu", query_unit, key_unit, precision=precise) * decay_mat
    attend = jnp.einsum("sthk,shkv->sthv", query_unit * growth[..., None], state, precision=precise)
    attend = attend + jnp.einsum("shtu,suhv->sthv", scores, update, precision=precise)
    final_cum = cumulative[:, -1:, :]
    fading = jnp.exp(final_cum - cumulative)
    new_state = jnp.exp(final_cum[:, 0, :])[:, :, None, None] * state
    new_state = new_state + jnp.einsum(
        "sthk,sthv->shkv", key_unit * fading[..., None], update, precision=precise
    )
    normed = attend * lax.rsqrt(jnp.mean(attend * attend, axis=-1, keepdims=True) + EPSILON)
    normed = normed * jax.nn.silu(gating) * live[:, :, None, None]
    mixed_heads = normed.reshape(seq_count * block_len, head_count * head_size).astype(jnp.bfloat16)
    return (mixed_heads, new_state)


def per_device(
    tokens,
    lengths,
    state,
    gain_first,
    first_gate,
    first_up,
    first_down,
    gain_mix,
    query_weight,
    key_weight,
    value_weight,
    gating_weight,
    write_weight,
    forget_weight,
    forget_rate,
    out_weight,
    gain_second,
    second_gate,
    second_up,
    second_down,
):
    after_first = feed_forward(tokens, gain_first, first_gate, first_up, first_down)
    seq_count = lengths.shape[0]
    own_count = seq_count * BLK
    whole_rows = lax.all_gather(after_first, ("kv", "tp"), axis=1, tiled=True)
    scaled_all = (whole_rows.astype(jnp.float32) * gain_mix).astype(jnp.bfloat16)
    stacked = jnp.stack(
        [
            jnp.dot(scaled_all, matrix, preferred_element_type=jnp.float32)
            for matrix in (query_weight, key_weight, value_weight, gating_weight)
        ]
    )
    owned = lax.all_to_all(
        stacked.astype(jnp.bfloat16), ("kv", "tp"), split_axis=1, concat_axis=2, tiled=True
    ).astype(stacked.dtype)
    row_start = lax.axis_index(("kv", "tp")) * own_count
    own_values = lax.dynamic_slice_in_dim(whole_rows, row_start, own_count, 0).astype(jnp.float32)
    own_scaled = lax.dynamic_slice_in_dim(scaled_all, row_start, own_count, 0)
    mix_scale = lax.rsqrt(jnp.mean(own_values * own_values, axis=1, keepdims=True) + EPSILON)
    query = (owned[0] * mix_scale).reshape(seq_count, BLK, HEADS, HEAD)
    key_in = (owned[1] * mix_scale).reshape(seq_count, BLK, HEADS, HEAD)
    value = (owned[2] * mix_scale).reshape(seq_count, BLK, HEADS, HEAD)
    gating = (owned[3] * mix_scale).reshape(seq_count, BLK, HEADS, HEAD)
    write_pre = (
        jnp.dot(own_scaled, write_weight, preferred_element_type=jnp.float32) * mix_scale
    ).reshape(seq_count, BLK, HEADS)
    forget_pre = (
        jnp.dot(own_scaled, forget_weight, preferred_element_type=jnp.float32) * mix_scale
    ).reshape(seq_count, BLK, HEADS)
    positions = jnp.arange(BLK, dtype=jnp.int32)
    live = (positions[None, :] < lengths[:, None]).astype(jnp.float32)
    mixed_heads, new_state = delta_block(
        query, key_in, value, gating, write_pre, forget_pre, forget_rate, live, state
    )
    half_cols = mixed_heads.shape[1] // 2
    portion = lax.all_gather(mixed_heads, ("kv", "tp"), axis=0, tiled=True)
    first_half = jnp.dot(
        portion[:, :half_cols], out_weight[:half_cols], preferred_element_type=jnp.float32
    ).astype(jnp.bfloat16)
    second_half = jnp.dot(
        portion[:, half_cols:], out_weight[half_cols:], preferred_element_type=jnp.float32
    ).astype(jnp.bfloat16)
    first_half, second_half = lax.optimization_barrier((first_half, second_half))
    mixed_sum = first_half.astype(jnp.float32) + second_half.astype(jnp.float32)
    after_mix = (after_first.astype(jnp.float32) + mixed_sum).astype(jnp.bfloat16)
    mixed_out = feed_forward(after_mix, gain_second, second_gate, second_up, second_down)
    return (mixed_out, new_state)


def solution(mesh):
    in_specs = (
        P("dp", ("kv", "tp")),
        P(("dp", "kv", "tp")),
        P(("dp", "kv", "tp"), None, None, None),
        P(),
        P(None, "kv"),
        P(None, "kv"),
        P("kv", None),
        P(),
        P(None, ("kv", "tp")),
        P(None, ("kv", "tp")),
        P(None, ("kv", "tp")),
        P(None, ("kv", "tp")),
        P(),
        P(),
        P(),
        P(None, ("kv", "tp")),
        P(),
        P(None, "kv"),
        P(None, "kv"),
        P("kv", None),
    )
    out_specs = (P("dp", ("kv", "tp")), P(("dp", "kv", "tp"), None, None, None))
    return jax.shard_map(
        per_device, mesh=mesh, in_specs=in_specs, out_specs=out_specs, check_vma=False
    )
```

profile of v0, /device:TPU:0, one launch (start us, length us, event | category | flops | bytes accessed | tf_op | source)
XLA Modules:
  0.0 174.8 jit_solution(16179178874863830319)
XLA Ops:
  7.2 4.8 %all_to_all.73 = bf16[2,32,256]{2,1,0:T(8,128)(2,1)S(1)} all-to-all(bf16[2,32,256]{2,1,0:T(8,128)(2,1)} %bitcast.150), channel_id=1, replica_groups=mesh['dp'=4,'kv'=4,'tp'=2] {'tp'}, dimensions={0} | all-to-all | bytes 65536 | tf_op jit(solution)/shard_map/all_to_all | solution.py:30
  12.0 15.1 %all_gather.12 = bf16[32,2048]{1,0:T(8,128)(2,1)S(1)} all-gather(bf16[32,512]{1,0:T(8,128)(2,1)S(1)} %bitcast.146), channel_id=1, replica_groups=mesh['dp'=4,'kv'=4,'tp'=2] {'kv'}, dimensions={1}, use_global_device_ids=true | all-gather | bytes 163840 | tf_op jit(solution)/shard_map/all_gather | solution.py:32
  27.1 0.1 fusion.25
  27.2 3.7 %convolution_multiply_fusion.3 = f32[32,1408]{1,0:T(8,128)S(1)} fusion(bf16[2048,1408]{1,0:T(8,128)(2,1)} %param.24, bf16[32,2048]{1,0:T(8,128)(2,1)S(1)} %all_gather.12, f32[2048]{0:T(1024)} %param.23, f32[32]{0:T(128)S(1)} %add_rsqrt_fusion.5), kind=kOutput, calls=%fused_computation.5 | convolution fusion | flops 184791040 | bytes 6086784 | tf_op jit(solution)/shard_map/dot_general | solution.py:16
  31.0 7.1 %fusion.21 = f32[32,2048]{1,0:T(8,128)} fusion(bf16[1408,2048]{1,0:T(8,128)(2,1)} %param.26, bf16[2048,1408]{1,0:T(8,128)(2,1)} %param.25, f32[32,1408]{1,0:T(8,128)S(1)} %convolution_multiply_fusion.3, bf16[32,2048]{1,0:T(8,128)(2,1)S(1)} %all_gather.12, f32[2048]{0:T(1024)S(1)} %copy-done.4, f32[32]{0:T(128)S(1)} %add_rsqrt_fusion.5), kind=kOutput, calls=%fused_computation.41 | convolution fusion | flops 369610752 | bytes 12116096 | tf_op jit(solution)/shard_map/dot_general | solution.py:25
  38.9 20.5 %reduce-scatter.3.cloned.1.call-done = f32[32,512]{1,0:T(8,128)} async-done(((f32[32,2048]{1,0:T(8,128)}), f32[32,512]{1,0:T(8,128)}) %reduce-scatter.3.cloned.1.call-update) | async-done | bytes 65552 | tf_op jit(solution)/shard_map/reduce_scatter | solution.py:35
  59.4 0.8 copy.159
  60.2 3.8 %all_to_all.74 = f32[32,2,256]{2,0,1:T(8,128)S(1)} all-to-all(f32[32,2,256]{2,0,1:T(8,128)S(1)} %bitcast.144), channel_id=1, replica_groups=mesh['dp'=4,'kv'=4,'tp'=2] {'tp'}, dimensions={1} | all-to-all | bytes 131072 | tf_op jit(solution)/shard_map/all_to_all | solution.py:36
  64.0 14.3 %all_gather.13 = bf16[64,2048]{1,0:T(8,128)(2,1)S(1)} all-gather(bf16[64,256]{1,0:T(8,128)(2,1)S(1)} %fusion.51), channel_id=1, replica_groups=mesh['dp'=4,'kv'=4,'tp'=2] {'kv','tp'}, dimensions={1}, use_global_device_ids=true | all-gather | bytes 294912 | tf_op jit(solution)/shard_map/all_gather | solution.py:117
  78.4 0.1 multiply_reduce_fusion.1
  78.6 0.3 fusion.12
  78.9 0.3 fusion.11
  79.2 1.5 fusion.10
  80.7 1.5 fusion.9
  82.3 0.8 copy.99
  83.0 3.4 %all-to-all-start.2 = ((bf16[4,64,256]{2,0,1:T(4,128)(2,1)}), bf16[4,64,256]{2,0,1:T(4,128)(2,1)S(1)}, u32[]{:S(2)}, u32[]{:S(2)}) async-start(bf16[4,64,256]{2,0,1:T(4,128)(2,1)} %copy.99), calls=%async_computation.3 | async-start | bytes 262144 | tf_op jit(solution)/shard_map/all_to_all | solution.py:125
  86.5 0.1 fusion.75
  86.7 0.9 fusion.80
  87.7 0.1 copy.104
  87.8 5.3 %all-to-all-done.2 = bf16[4,64,256]{2,0,1:T(4,128)(2,1)S(1)} async-done(((bf16[4,64,256]{2,0,1:T(4,128)(2,1)}), bf16[4,64,256]{2,0,1:T(4,128)(2,1)S(1)}, u32[]{:S(2)}, u32[]{:S(2)}) %all-to-all-start.2) | async-done | bytes 131104 | tf_op jit(solution)/shard_map/all_to_all | solution.py:125
  93.1 0.1 copy.157
  93.3 0.2 fusion.58
  93.6 0.2 fusion.67
  93.8 0.3 fusion.8
  94.1 0.3 fusion.88
  94.3 0.2 fusion.62
  94.6 0.3 convolution_add_fusion.1
  94.8 0.3 convolution_multiply_fusion.4
  95.2 0.3 fusion.89
  95.5 0.2 convolution_bitcast_fusion.2
  95.7 0.2 fusion.55
  96.0 1.0 convolution_bitcast_fusion.3
  96.9 1.0 fusion.7
  97.9 0.3 multiply_reduce_fusion
  98.4 0.1 fusion.70
  98.5 14.2 %all_gather.14 = bf16[64,2048]{1,0:T(8,128)(2,1)S(1)} all-gather(bf16[8,2048]{1,0:T(8,128)(2,1)S(1)} %fusion.70), channel_id=1, replica_groups=mesh['dp'=4,'kv'=4,'tp'=2] {'kv','tp'}, dimensions={0}, use_global_device_ids=true | all-gather | bytes 294912 | tf_op jit(solution)/shard_map/all_gather | solution.py:148
  112.8 1.2 convolution_convert_fusion
  114.0 1.2 convolution_convert_fusion.1
  115.3 3.7 %all_to_all.75 = bf16[2,32,256]{2,1,0:T(8,128)(2,1)S(1)} all-to-all(bf16[2,32,256]{2,1,0:T(8,128)(2,1)S(1)} %bitcast.143), channel_id=1, replica_groups=mesh['dp'=4,'kv'=4,'tp'=2] {'tp'}, dimensions={0} | all-to-all | bytes 65536 | tf_op jit(solution)/shard_map/all_to_all | solution.py:30
  119.0 13.6 %all_gather.15 = bf16[32,2048]{1,0:T(8,128)(2,1)S(1)} all-gather(bf16[32,512]{1,0:T(8,128)(2,1)S(1)} %bitcast.147), channel_id=1, replica_groups=mesh['dp'=4,'kv'=4,'tp'=2] {'kv'}, dimensions={1}, use_global_device_ids=true | all-gather | bytes 163840 | tf_op jit(solution)/shard_map/all_gather | solution.py:32
  132.6 0.1 fusion.27
  132.7 3.6 %convolution_multiply_fusion.1 = f32[32,1408]{1,0:T(8,128)S(1)} fusion(bf16[2048,1408]{1,0:T(8,128)(2,1)} %param.37, bf16[32,2048]{1,0:T(8,128)(2,1)S(1)} %all_gather.15, f32[2048]{0:T(1024)S(1)} %copy-done.5, f32[32]{0:T(128)S(1)} %add_rsqrt_fusion.3), kind=kOutput, calls=%fused_computation.2 | convolution fusion | flops 184791040 | bytes 6086784 | tf_op jit(solution)/shard_map/dot_general | solution.py:16
  136.4 7.0 %fusion.20 = f32[32,2048]{1,0:T(8,128)} fusion(bf16[1408,2048]{1,0:T(8,128)(2,1)} %param.39, bf16[2048,1408]{1,0:T(8,128)(2,1)} %param.38, f32[32,1408]{1,0:T(8,128)S(1)} %convolution_multiply_fusion.1, bf16[32,2048]{1,0:T(8,128)(2,1)S(1)} %all_gather.15, f32[2048]{0:T(1024)S(1)} %copy-done.5, f32[32]{0:T(128)S(1)} %add_rsqrt_fusion.3), kind=kOutput, calls=%fused_computation.40 | convolution fusion | flops 369610752 | bytes 12116096 | tf_op jit(solution)/shard_map/dot_general | solution.py:25
  143.5 2.8 %fusion.4 = f32[1,16,128,128]{3,2,1,0:T(8,128)} fusion(f32[8,16,128]{2,0,1:T(8,128)S(1)} %fusion.7, f32[1,16,128,128]{3,2,1,0:T(8,128)S(1)} %copy-done.1, f32[16]{0:T(128)S(1)} %fusion.86, f32[8,16,128]{2,1,0:T(8,128)S(1)} %get-tuple-element.20), kind=kOutput, calls=%fused_computation.9 | convolution fusion | flops 25690112 | bytes 2228288 | tf_op jit(solution)/shard_map/sthk,sthv->shkv/dot_general | solution.py:83
  146.3 16.4 %reduce-scatter.5.cloned.1.call-done = f32[32,512]{1,0:T(8,128)} async-done(((f32[32,2048]{1,0:T(8,128)}), f32[32,512]{1,0:T(8,128)}) %reduce-scatter.5.cloned.1.call-update) | async-done | bytes 65552 | tf_op jit(solution)/shard_map/reduce_scatter | solution.py:35
  162.7 0.8 copy.158
  163.6 3.8 %all_to_all.76 = f32[32,2,256]{2,0,1:T(8,128)S(1)} all-to-all(f32[32,2,256]{2,0,1:T(8,128)S(1)} %bitcast.145), channel_id=1, replica_groups=mesh['dp'=4,'kv'=4,'tp'=2] {'tp'}, dimensions={1} | all-to-all | bytes 131072 | tf_op jit(solution)/shard_map/all_to_all | solution.py:36
  167.4 0.6 fusion.50
  (55 shorter events, 0.9 us)
Async XLA Ops:
  7.2 71.4 %copy-start = (bf16[2048,256]{1,0:T(8,128)(2,1)S(1)}, bf16[2048,256]{1,0:T(8,128)(2,1)}, u32[]{:S(2)}) copy-start(bf16[2048,256]{1,0:T(8,128)(2,1)} %param.31) | copy-start | bytes 3145732
  7.2 23.7 %copy-start.4 = (f32[2048]{0:T(1024)S(1)}, f32[2048]{0:T(1024)}, u32[]{:S(2)}) copy-start(f32[2048]{0:T(1024)} %param.23) | copy-start | bytes 24580
  7.2 52.2 %reduce-scatter.3.cloned.1.call-start = ((), (), s32[]{:S(2)}) async-start(), calls=%async_computation.7 | async-start | bytes 327680 | tf_op jit(solution)/shard_map/reduce_scatter | solution.py:35
  30.9 7.9 %copy-start.8 = (f32[16]{0:T(128)S(1)}, f32[16]{0:T(128)}, u32[]{:S(2)}) copy-start(f32[16]{0:T(128)} %param.34) | copy-start | bytes 196
  30.9 33.1 %copy-start.3 = (bf16[64,256]{1,0:T(8,128)(2,1)S(1)}, bf16[64,256]{1,0:T(8,128)(2,1)}, u32[]{:S(2)}) copy-start(bf16[64,256]{1,0:T(8,128)(2,1)} %param.20) | copy-start | bytes 98308
  30.9 47.6 %copy-start.6 = (f32[2048]{0:T(1024)S(1)}, f32[2048]{0:T(1024)}, u32[]{:S(2)}) copy-start(f32[2048]{0:T(1024)} %param.27) | copy-start | bytes 24580
  30.9 47.9 %copy-start.2 = (bf16[2048,256]{1,0:T(8,128)(2,1)S(1)}, bf16[2048,256]{1,0:T(8,128)(2,1)}, u32[]{:S(2)}) copy-start(bf16[2048,256]{1,0:T(8,128)(2,1)} %param.30) | copy-start | bytes 3145732
  38.1 48.4 %copy-start.7 = (bf16[2048,16]{0,1:T(8,128)(2,1)S(1)}, bf16[2048,16]{0,1:T(8,128)(2,1)}, u32[]{:S(2)}) copy-start(bf16[2048,16]{0,1:T(8,128)(2,1)} %param.33) | copy-start | bytes 196612
  64.0 31.9 %copy-start.1 = (f32[1,16,128,128]{3,2,1,0:T(8,128)S(1)}, f32[1,16,128,128]{3,2,1,0:T(8,128)}, u32[]{:S(2)}) copy-start(f32[1,16,128,128]{3,2,1,0:T(8,128)} %param.22) | copy-start | bytes 3145732
  80.7 52.0 %copy-start.5 = (f32[2048]{0:T(1024)S(1)}, f32[2048]{0:T(1024)}, u32[]{:S(2)}) copy-start(f32[2048]{0:T(1024)} %param.36) | copy-start | bytes 24580
  83.0 10.1 %all-to-all-start.2 = ((bf16[4,64,256]{2,0,1:T(4,128)(2,1)}), bf16[4,64,256]{2,0,1:T(4,128)(2,1)S(1)}, u32[]{:S(2)}, u32[]{:S(2)}) async-start(bf16[4,64,256]{2,0,1:T(4,128)(2,1)} %copy.99), calls=%async_computation.3 | async-start | bytes 262144 | tf_op jit(solution)/shard_map/all_to_all | solution.py:125
  86.4 76.3 %reduce-scatter.5.cloned.1.call-start = ((), (), s32[]{:S(2)}) async-start(), calls=%async_computation.8 | async-start | bytes 327680 | tf_op jit(solution)/shard_map/reduce_scatter | solution.py:35
Sparse Core Ops, SparseCore 0:
  38.2 21.0 reduce-scatter.2
  143.6 19.1 reduce-scatter.4
where the time goes:
time: 176 us; the launch traced here: 175 us
  blocking collectives  73.2 us (42%)
  waiting for transfers between devices  42.3 us (24%)
  matrix products  35.8 us (20%)
  between operations  15.2 us (9%)
  starting transfers between devices  3.45 us (2%)
  local copies, waits for them, and re-layouts  3.13 us (2%)
  other arithmetic  1.76 us (1%)
    reduce_scatter x2, waiting for transfers between devices, feed_forward(): lax.psum_scatter(ffn_term, 'kv', scatter_dimension=1, tiled=True)  36.9 us
    all_gather x2, blocking collectives, feed_forward(): lax.all_gather(paired, 'kv', axis=1, tiled=True)  28.6 us
    all_gather x1, blocking collectives, per_device(): whole_rows = lax.all_gather(after_first, ('kv', 'tp'), axis=1, tiled=True)  14.3 us
    all_gather x1, blocking collectives, per_device(): portion = lax.all_gather(mixed_heads, ('kv', 'tp'), axis=0, tiled=True)  14.2 us
    dot_general x2, matrix products, finish_units(): return jnp.dot(hidden, down_rows, preferred_element_type=jnp.float32)  14.2 us
    all_to_all x2, blocking collectives, feed_forward(): lax.all_to_all(hidden_in, 'tp', split_axis=0, concat_axis=1, tiled=True)  8.52 us
    all_to_all x2, blocking collectives, feed_forward(): lax.all_to_all(partial_value, 'tp', split_axis=1, concat_axis=0, tiled=True)  7.56 us
    dot_general x2, matrix products, fold_step(): gate_acc = jnp.dot(scaled, gate_cols, preferred_element_type=jnp.float32)  7.31 us
  transfers between devices with their start and end apart: 3, of which 3 were waited for; matrix products, arithmetic and copies ran while one was open for 2% of the time, Pallas kernels for 0%

commit v1 on v0

--- a/solution.py
+++ b/solution.py
@@ -8,6 +8,27 @@
 HEAD = 128
 BLK = 8
 EPSILON = 1e-06
+
+
+def ring_gather(x, axis, dim):
+    count, place, rows = (lax.axis_size(axis), lax.axis_index(axis), x.shape[dim])
+    ahead = [(i, (i + 1) % count) for i in range(count)]
+    left = [(i, (i - 1) % count) for i in range(count)]
+    out = jnp.zeros((*x.shape[:dim], count * rows, *x.shape[dim + 1 :]), x.dtype)
+    out = lax.dynamic_update_slice_in_dim(out, x, place * rows, axis=dim)
+    from_left = from_right = x
+    half = count // 2
+    for hop in range(1, half + 1):
+        from_left = lax.ppermute(from_left, axis, ahead)
+        out = lax.dynamic_update_slice_in_dim(
+            out, from_left, (place - hop) % count * rows, axis=dim
+        )
+        if hop < count - half:
+            from_right = lax.ppermute(from_right, axis, left)
+            out = lax.dynamic_update_slice_in_dim(
+                out, from_right, (place + hop) % count * rows, axis=dim
+            )
+    return out
 
 
 def fold_step(gain, gate_cols, up_cols, portion):
@@ -114,7 +135,7 @@
     after_first = feed_forward(tokens, gain_first, first_gate, first_up, first_down)
     seq_count = lengths.shape[0]
     own_count = seq_count * BLK
-    whole_rows = lax.all_gather(after_first, ("kv", "tp"), axis=1, tiled=True)
+    whole_rows = ring_gather(after_first, ("kv", "tp"), 1)
     scaled_all = (whole_rows.astype(jnp.float32) * gain_mix).astype(jnp.bfloat16)
     stacked = jnp.stack(
         [

time: 176 us -> 183 us (1.040)
  blocking collectives: 73.2 us -> 58.9 us
  starting transfers between devices: 3.45 us -> 14.2 us
  waiting for transfers between devices: 42.3 us -> 52.9 us
    all_gather x1 -> x0, blocking collectives: 14.3 us -> none  [per_device(): whole_rows = lax.all_gather(after_first, ('kv', 'tp'), axis=1, tiled=True)]
    ppermute x0 -> x7, starting transfers between devices: none -> 10.8 us  [the longest x3 10.6 us: ring_gather(): from_right = lax.ppermute(from_right, axis, left)]
    ppermute x0 -> x7, waiting for transfers between devices: none -> 9.8 us  [the longest x4 9.71 us: ring_gather(): from_left = lax.ppermute(from_left, axis, ahead)]
  transfers between devices with their start and end apart: 3 -> 10, of which waited for: 3 -> 8; matrix products, arithmetic and copies ran while one was open for 2% -> 2% of each run, Pallas kernels for 0% -> 0%
where the time goes in v1:
time: 183 us; the launch traced here: 182 us
  blocking collectives  58.9 us (32%)
  waiting for transfers between devices  52.9 us (29%)
  matrix products  36.1 us (20%)
  between operations  15.2 us (8%)
  starting transfers between devices  14.2 us (8%)
  local copies, waits for them, and re-layouts  3.13 us (2%)
    reduce_scatter x2, waiting for transfers between devices, feed_forward(): lax.psum_scatter(ffn_term, 'kv', scatter_dimension=1, tiled=True)  36.9 us
    all_gather x2, blocking collectives, feed_forward(): lax.all_gather(paired, 'kv', axis=1, tiled=True)  28.6 us
    all_gather x1, blocking collectives, per_device(): portion = lax.all_gather(mixed_heads, ('kv', 'tp'), axis=0, tiled=True)  14.2 us
    dot_general x2, matrix products, finish_units(): return jnp.dot(hidden, down_rows, preferred_element_type=jnp.float32)  14.1 us
    ppermute x3, starting transfers between devices, ring_gather(): from_right = lax.ppermute(from_right, axis, left)  10.6 us
    ppermute x4, waiting for transfers between devices, ring_gather(): from_left = lax.ppermute(from_left, axis, ahead)  9.71 us
    all_to_all x2, blocking collectives, feed_forward(): lax.all_to_all(hidden_in, 'tp', split_axis=0, concat_axis=1, tiled=True)  8.52 us
    all_to_all x2, blocking collectives, feed_forward(): lax.all_to_all(partial_value, 'tp', split_axis=1, concat_axis=0, tiled=True)  7.56 us
  transfers between devices with their start and end apart: 10, of which 8 were waited for; matrix products, arithmetic and copies ran while one was open for 2% of the time, Pallas kernels for 0%

profile of v1, /device:TPU:0, one launch (start us, length us, event | category | flops | bytes accessed | tf_op | source)
XLA Modules:
  0.0 182.2 jit_solution(6646317066628369878)
XLA Ops:
  7.2 4.8 %all_to_all.73 = bf16[2,32,256]{2,1,0:T(8,128)(2,1)S(1)} all-to-all(bf16[2,32,256]{2,1,0:T(8,128)(2,1)} %bitcast.146), channel_id=1, replica_groups=mesh['dp'=4,'kv'=4,'tp'=2] {'tp'}, dimensions={0} | all-to-all | bytes 65536 | tf_op jit(solution)/shard_map/all_to_all | solution.py:51
  12.0 15.1 %all_gather.9 = bf16[32,2048]{1,0:T(8,128)(2,1)S(1)} all-gather(bf16[32,512]{1,0:T(8,128)(2,1)S(1)} %bitcast.147), channel_id=1, replica_groups=mesh['dp'=4,'kv'=4,'tp'=2] {'kv'}, dimensions={1}, use_global_device_ids=true | all-gather | bytes 163840 | tf_op jit(solution)/shard_map/all_gather | solution.py:53
  27.2 3.7 %convolution_multiply_fusion.3 = f32[32,1408]{1,0:T(8,128)S(1)} fusion(bf16[2048,1408]{1,0:T(8,128)(2,1)} %param.24, bf16[32,2048]{1,0:T(8,128)(2,1)S(1)} %all_gather.9, f32[2048]{0:T(1024)} %param.23, f32[32]{0:T(128)S(1)} %add_rsqrt_fusion.5), kind=kOutput, calls=%fused_computation.5 | convolution fusion | flops 184791040 | bytes 6086784 | tf_op jit(solution)/shard_map/dot_general | solution.py:37
  30.9 7.1 %fusion.21 = f32[32,2048]{1,0:T(8,128)} fusion(bf16[1408,2048]{1,0:T(8,128)(2,1)} %param.26, bf16[2048,1408]{1,0:T(8,128)(2,1)} %param.25, f32[32,1408]{1,0:T(8,128)S(1)} %convolution_multiply_fusion.3, bf16[32,2048]{1,0:T(8,128)(2,1)S(1)} %all_gather.9, f32[2048]{0:T(1024)S(1)} %copy-done.3, f32[32]{0:T(128)S(1)} %add_rsqrt_fusion.5), kind=kOutput, calls=%fused_computation.41 | convolution fusion | flops 369610752 | bytes 12116096 | tf_op jit(solution)/shard_map/dot_general | solution.py:46
  38.8 20.5 %reduce-scatter.3.cloned.1.call-done = f32[32,512]{1,0:T(8,128)} async-done(((f32[32,2048]{1,0:T(8,128)}), f32[32,512]{1,0:T(8,128)}) %reduce-scatter.3.cloned.1.call-update) | async-done | bytes 65552 | tf_op jit(solution)/shard_map/reduce_scatter | solution.py:56
  59.3 0.8 copy.159
  60.1 3.8 %all_to_all.74 = f32[32,2,256]{2,0,1:T(8,128)S(1)} all-to-all(f32[32,2,256]{2,0,1:T(8,128)S(1)} %bitcast.144), channel_id=1, replica_groups=mesh['dp'=4,'kv'=4,'tp'=2] {'tp'}, dimensions={1} | all-to-all | bytes 131072 | tf_op jit(solution)/shard_map/all_to_all | solution.py:57
  64.0 0.2 collective-permute-start
  64.2 3.4 %collective-permute-start.1 = (bf16[64,256]{1,0:T(8,128)(2,1)S(1)}, bf16[64,256]{1,0:T(8,128)(2,1)S(1)}, u32[]{:S(2)}, u32[]{:S(2)}) collective-permute-start(bf16[64,256]{1,0:T(8,128)(2,1)S(1)} %get-tuple-element.23), channel_id=1, source_target_pairs={{0,7},{1,0},{2,1},{3,2},{4,3},{5,4},{6,5},{7,6},{8,15},{9,8},{10,9... | collective-permute-start | bytes 98312 | tf_op jit(solution)/shard_map/ppermute | solution.py:27
  67.6 1.6 collective-permute-done
  69.2 3.5 %collective-permute-start.3 = (bf16[64,256]{1,0:T(8,128)(2,1)S(1)}, bf16[64,256]{1,0:T(8,128)(2,1)S(1)}, u32[]{:S(2)}, u32[]{:S(2)}) collective-permute-start(bf16[64,256]{1,0:T(8,128)(2,1)S(1)} %collective-permute-done.1), channel_id=1, source_target_pairs={{0,7},{1,0},{2,1},{3,2},{4,3},{5,4},{6,5},{7,6},{8,15},{9,8},{10,9... | collective-permute-start | bytes 98312 | tf_op jit(solution)/shard_map/ppermute | solution.py:27
  72.7 1.6 collective-permute-done.2
  74.3 3.6 %collective-permute-start.5 = (bf16[64,256]{1,0:T(8,128)(2,1)S(1)}, bf16[64,256]{1,0:T(8,128)(2,1)S(1)}, u32[]{:S(2)}, u32[]{:S(2)}) collective-permute-start(bf16[64,256]{1,0:T(8,128)(2,1)S(1)} %collective-permute-done.3), channel_id=1, source_target_pairs={{0,7},{1,0},{2,1},{3,2},{4,3},{5,4},{6,5},{7,6},{8,15},{9,8},{10,9... | collective-permute-start | bytes 98312 | tf_op jit(solution)/shard_map/ppermute | solution.py:27
  78.0 1.5 collective-permute-done.4
  79.6 5.0 %collective-permute-done.6 = bf16[64,256]{1,0:T(8,128)(2,1)S(1)} collective-permute-done((bf16[64,256]{1,0:T(8,128)(2,1)S(1)}, bf16[64,256]{1,0:T(8,128)(2,1)S(1)}, u32[]{:S(2)}, u32[]{:S(2)}) %collective-permute-start.6) | collective-permute-done | bytes 32800 | tf_op jit(solution)/shard_map/ppermute | solution.py:22
  84.8 0.3 fusion.12
  85.1 1.5 fusion.11
  86.6 1.5 fusion.10
  88.2 1.5 fusion.9
  89.7 0.8 copy.99
  90.5 3.4 %all-to-all-start.2 = ((bf16[4,64,256]{2,0,1:T(4,128)(2,1)}), bf16[4,64,256]{2,0,1:T(4,128)(2,1)S(1)}, u32[]{:S(2)}, u32[]{:S(2)}) async-start(bf16[4,64,256]{2,0,1:T(4,128)(2,1)} %copy.99), calls=%async_computation.3 | async-start | bytes 262144 | tf_op jit(solution)/shard_map/all_to_all | solution.py:146
  93.9 0.1 fusion.75
  94.4 6.2 %all-to-all-done.2 = bf16[4,64,256]{2,0,1:T(4,128)(2,1)S(1)} async-done(((bf16[4,64,256]{2,0,1:T(4,128)(2,1)}), bf16[4,64,256]{2,0,1:T(4,128)(2,1)S(1)}, u32[]{:S(2)}, u32[]{:S(2)}) %all-to-all-start.2) | async-done | bytes 131104 | tf_op jit(solution)/shard_map/all_to_all | solution.py:146
  100.7 0.2 fusion.58
  101.1 0.2 fusion.67
  101.3 0.3 fusion.8
  101.5 0.2 fusion.88
  101.8 0.2 fusion.62
  102.0 0.3 convolution_add_fusion.1
  102.3 0.3 convolution_multiply_fusion.4
  102.7 0.2 fusion.89
  102.9 0.2 convolution_bitcast_fusion.2
  103.2 0.2 fusion.55
  103.4 1.0 convolution_bitcast_fusion.3
  104.4 1.0 fusion.7
  105.4 0.3 multiply_reduce_fusion
  106.0 14.2 %all_gather.10 = bf16[64,2048]{1,0:T(8,128)(2,1)S(1)} all-gather(bf16[8,2048]{1,0:T(8,128)(2,1)S(1)} %fusion.70), channel_id=1, replica_groups=mesh['dp'=4,'kv'=4,'tp'=2] {'kv','tp'}, dimensions={0}, use_global_device_ids=true | all-gather | bytes 294912 | tf_op jit(solution)/shard_map/all_gather | solution.py:169
  120.2 1.2 convolution_convert_fusion
  121.5 1.2 convolution_convert_fusion.1
  122.7 3.7 %all_to_all.75 = bf16[2,32,256]{2,1,0:T(8,128)(2,1)S(1)} all-to-all(bf16[2,32,256]{2,1,0:T(8,128)(2,1)S(1)} %bitcast.143), channel_id=1, replica_groups=mesh['dp'=4,'kv'=4,'tp'=2] {'tp'}, dimensions={0} | all-to-all | bytes 65536 | tf_op jit(solution)/shard_map/all_to_all | solution.py:51
  126.5 13.6 %all_gather.11 = bf16[32,2048]{1,0:T(8,128)(2,1)S(1)} all-gather(bf16[32,512]{1,0:T(8,128)(2,1)S(1)} %bitcast.148), channel_id=1, replica_groups=mesh['dp'=4,'kv'=4,'tp'=2] {'kv'}, dimensions={1}, use_global_device_ids=true | all-gather | bytes 163840 | tf_op jit(solution)/shard_map/all_gather | solution.py:53
  140.2 3.6 %convolution_multiply_fusion.1 = f32[32,1408]{1,0:T(8,128)S(1)} fusion(bf16[2048,1408]{1,0:T(8,128)(2,1)} %param.37, bf16[32,2048]{1,0:T(8,128)(2,1)S(1)} %all_gather.11, f32[2048]{0:T(1024)S(1)} %copy-done.4, f32[32]{0:T(128)S(1)} %add_rsqrt_fusion.3), kind=kOutput, calls=%fused_computation.2 | convolution fusion | flops 184791040 | bytes 6086784 | tf_op jit(solution)/shard_map/dot_general | solution.py:37
  143.8 7.0 %fusion.20 = f32[32,2048]{1,0:T(8,128)} fusion(bf16[1408,2048]{1,0:T(8,128)(2,1)} %param.39, bf16[2048,1408]{1,0:T(8,128)(2,1)} %param.38, f32[32,1408]{1,0:T(8,128)S(1)} %convolution_multiply_fusion.1, bf16[32,2048]{1,0:T(8,128)(2,1)S(1)} %all_gather.11, f32[2048]{0:T(1024)S(1)} %copy-done.4, f32[32]{0:T(128)S(1)} %add_rsqrt_fusion.3), kind=kOutput, calls=%fused_computation.40 | convolution fusion | flops 369610752 | bytes 12116096 | tf_op jit(solution)/shard_map/dot_general | solution.py:46
  150.9 2.8 %fusion.4 = f32[1,16,128,128]{3,2,1,0:T(8,128)} fusion(f32[8,16,128]{2,0,1:T(8,128)S(1)} %fusion.7, f32[1,16,128,128]{3,2,1,0:T(8,128)S(1)} %copy-done.1, f32[16]{0:T(128)S(1)} %fusion.86, f32[8,16,128]{2,1,0:T(8,128)S(1)} %get-tuple-element.20), kind=kOutput, calls=%fused_computation.9 | convolution fusion | flops 25690112 | bytes 2228288 | tf_op jit(solution)/shard_map/sthk,sthv->shkv/dot_general | solution.py:104
  153.8 16.4 %reduce-scatter.5.cloned.1.call-done = f32[32,512]{1,0:T(8,128)} async-done(((f32[32,2048]{1,0:T(8,128)}), f32[32,512]{1,0:T(8,128)}) %reduce-scatter.5.cloned.1.call-update) | async-done | bytes 65552 | tf_op jit(solution)/shard_map/reduce_scatter | solution.py:56
  170.1 0.8 copy.158
  171.0 3.8 %all_to_all.76 = f32[32,2,256]{2,0,1:T(8,128)S(1)} all-to-all(f32[32,2,256]{2,0,1:T(8,128)S(1)} %bitcast.145), channel_id=1, replica_groups=mesh['dp'=4,'kv'=4,'tp'=2] {'tp'}, dimensions={1} | all-to-all | bytes 131072 | tf_op jit(solution)/shard_map/all_to_all | solution.py:57
  174.8 0.6 fusion.50
  (76 shorter events, 1.8 us)
Async XLA Ops:
  7.2 77.6 %copy-start = (bf16[2048,256]{1,0:T(8,128)(2,1)S(1)}, bf16[2048,256]{1,0:T(8,128)(2,1)}, u32[]{:S(2)}) copy-start(bf16[2048,256]{1,0:T(8,128)(2,1)} %param.31) | copy-start | bytes 3145732
  7.2 23.7 %copy-start.3 = (f32[2048]{0:T(1024)S(1)}, f32[2048]{0:T(1024)}, u32[]{:S(2)}) copy-start(f32[2048]{0:T(1024)} %param.23) | copy-start | bytes 24580
  7.2 52.1 %reduce-scatter.3.cloned.1.call-start = ((), (), s32[]{:S(2)}) async-start(), calls=%async_computation.7 | async-start | bytes 327680 | tf_op jit(solution)/shard_map/reduce_scatter | solution.py:56
  30.9 7.8 %copy-start.8 = (f32[16]{0:T(128)S(1)}, f32[16]{0:T(128)}, u32[]{:S(2)}) copy-start(f32[16]{0:T(128)} %param.34) | copy-start | bytes 196
  30.9 33.0 %copy-start.2 = (bf16[64,256]{1,0:T(8,128)(2,1)S(1)}, bf16[64,256]{1,0:T(8,128)(2,1)}, u32[]{:S(2)}) copy-start(bf16[64,256]{1,0:T(8,128)(2,1)} %param.20) | copy-start | bytes 98308
  30.9 53.8 %copy-start.5 = (f32[2048]{0:T(1024)S(1)}, f32[2048]{0:T(1024)}, u32[]{:S(2)}) copy-start(f32[2048]{0:T(1024)} %param.27) | copy-start | bytes 24580
  38.0 55.9 %copy-start.6 = (bf16[2048,16]{0,1:T(8,128)(2,1)S(1)}, bf16[2048,16]{0,1:T(8,128)(2,1)}, u32[]{:S(2)}) copy-start(bf16[2048,16]{0,1:T(8,128)(2,1)} %param.33) | copy-start | bytes 196612
  38.0 56.2 %copy-start.7 = (bf16[2048,16]{0,1:T(8,128)(2,1)S(1)}, bf16[2048,16]{0,1:T(8,128)(2,1)}, u32[]{:S(2)}) copy-start(bf16[2048,16]{0,1:T(8,128)(2,1)} %param.32) | copy-start | bytes 196612
  64.0 5.2 %collective-permute-start = (bf16[64,256]{1,0:T(8,128)(2,1)S(1)}, bf16[64,256]{1,0:T(8,128)(2,1)S(1)}, u32[]{:S(2)}, u32[]{:S(2)}) collective-permute-start(bf16[64,256]{1,0:T(8,128)(2,1)S(1)} %get-tuple-element.23), channel_id=1, source_target_pairs={{0,1},{1,2},{2,3},{3,4},{4,5},{5,6},{6,7},{7,0},{8,9},{9,10},{10,1... | collective-permute-start | bytes 98312 | tf_op jit(solution)/shard_map/ppermute | solution.py:22
  64.2 5.0 %collective-permute-start.1 = (bf16[64,256]{1,0:T(8,128)(2,1)S(1)}, bf16[64,256]{1,0:T(8,128)(2,1)S(1)}, u32[]{:S(2)}, u32[]{:S(2)}) collective-permute-start(bf16[64,256]{1,0:T(8,128)(2,1)S(1)} %get-tuple-element.23), channel_id=1, source_target_pairs={{0,7},{1,0},{2,1},{3,2},{4,3},{5,4},{6,5},{7,6},{8,15},{9,8},{10,9... | collective-permute-start | bytes 98312 | tf_op jit(solution)/shard_map/ppermute | solution.py:27
  69.2 5.2 %collective-permute-start.2 = (bf16[64,256]{1,0:T(8,128)(2,1)S(1)}, bf16[64,256]{1,0:T(8,128)(2,1)S(1)}, u32[]{:S(2)}, u32[]{:S(2)}) collective-permute-start(bf16[64,256]{1,0:T(8,128)(2,1)S(1)} %collective-permute-done), channel_id=1, source_target_pairs={{0,1},{1,2},{2,3},{3,4},{4,5},{5,6},{6,7},{7,0},{8,9},{9,10},{10,1... | collective-permute-start | bytes 98312 | tf_op jit(solution)/shard_map/ppermute | solution.py:22
  69.2 5.2 %collective-permute-start.3 = (bf16[64,256]{1,0:T(8,128)(2,1)S(1)}, bf16[64,256]{1,0:T(8,128)(2,1)S(1)}, u32[]{:S(2)}, u32[]{:S(2)}) collective-permute-start(bf16[64,256]{1,0:T(8,128)(2,1)S(1)} %collective-permute-done.1), channel_id=1, source_target_pairs={{0,7},{1,0},{2,1},{3,2},{4,3},{5,4},{6,5},{7,6},{8,15},{9,8},{10,9... | collective-permute-start | bytes 98312 | tf_op jit(solution)/shard_map/ppermute | solution.py:27
  74.3 5.1 %collective-permute-start.4 = (bf16[64,256]{1,0:T(8,128)(2,1)S(1)}, bf16[64,256]{1,0:T(8,128)(2,1)S(1)}, u32[]{:S(2)}, u32[]{:S(2)}) collective-permute-start(bf16[64,256]{1,0:T(8,128)(2,1)S(1)} %collective-permute-done.2), channel_id=1, source_target_pairs={{0,1},{1,2},{2,3},{3,4},{4,5},{5,6},{6,7},{7,0},{8,9},{9,10},{10,1... | collective-permute-start | bytes 98312 | tf_op jit(solution)/shard_map/ppermute | solution.py:22
  74.3 5.2 %collective-permute-start.5 = (bf16[64,256]{1,0:T(8,128)(2,1)S(1)}, bf16[64,256]{1,0:T(8,128)(2,1)S(1)}, u32[]{:S(2)}, u32[]{:S(2)}) collective-permute-start(bf16[64,256]{1,0:T(8,128)(2,1)S(1)} %collective-permute-done.3), channel_id=1, source_target_pairs={{0,7},{1,0},{2,1},{3,2},{4,3},{5,4},{6,5},{7,6},{8,15},{9,8},{10,9... | collective-permute-start | bytes 98312 | tf_op jit(solution)/shard_map/ppermute | solution.py:27
  78.0 25.4 %copy-start.1 = (f32[1,16,128,128]{3,2,1,0:T(8,128)S(1)}, f32[1,16,128,128]{3,2,1,0:T(8,128)}, u32[]{:S(2)}) copy-start(f32[1,16,128,128]{3,2,1,0:T(8,128)} %param.22) | copy-start | bytes 3145732
  79.5 5.1 %collective-permute-start.6 = (bf16[64,256]{1,0:T(8,128)(2,1)S(1)}, bf16[64,256]{1,0:T(8,128)(2,1)S(1)}, u32[]{:S(2)}, u32[]{:S(2)}) collective-permute-start(bf16[64,256]{1,0:T(8,128)(2,1)S(1)} %collective-permute-done.4), channel_id=1, source_target_pairs={{0,1},{1,2},{2,3},{3,4},{4,5},{5,6},{6,7},{7,0},{8,9},{9,10},{10,1... | collective-permute-start | bytes 98312 | tf_op jit(solution)/shard_map/ppermute | solution.py:22
  88.2 52.0 %copy-start.4 = (f32[2048]{0:T(1024)S(1)}, f32[2048]{0:T(1024)}, u32[]{:S(2)}) copy-start(f32[2048]{0:T(1024)} %param.36) | copy-start | bytes 24580
  90.5 10.1 %all-to-all-start.2 = ((bf16[4,64,256]{2,0,1:T(4,128)(2,1)}), bf16[4,64,256]{2,0,1:T(4,128)(2,1)S(1)}, u32[]{:S(2)}, u32[]{:S(2)}) async-start(bf16[4,64,256]{2,0,1:T(4,128)(2,1)} %copy.99), calls=%async_computation.3 | async-start | bytes 262144 | tf_op jit(solution)/shard_map/all_to_all | solution.py:146
  93.9 76.3 %reduce-scatter.5.cloned.1.call-start = ((), (), s32[]{:S(2)}) async-start(), calls=%async_computation.8 | async-start | bytes 327680 | tf_op jit(solution)/shard_map/reduce_scatter | solution.py:56
Sparse Core Ops, SparseCore 0:
  38.2 21.0 reduce-scatter.2
  151.0 19.0 reduce-scatter.4
